TPU v7x, 32 devices: a whole 2x2x4 slice. The times are simulated.
32 devices in a mesh: ep: 8 (over z, core), tp: 4 (over y, x).
Axes of the slice: x: 2, y: 2, z: 4, core: 2. Of those that a mesh axis runs over, the one named last changes fastest.
Arguments:
- tokens: bfloat16 [128, 2048], P('ep'), may hold values from -6 to 6
- old_state: float32 [128, 16, 128, 128], P('ep', 'tp'), may hold values from -2 to 2
- lower_bound: float32 [2048], P('tp'), may hold values from 0.05 to 0.95
- head_gain: float32 [2048], P('tp'), may hold values from 0.1 to 1.9
- norm_gains: float32 [4, 2048], replicated, may hold values from 0.1 to 1.9
- w_query: bfloat16 [2048, 2048], P('ep', 'tp'), may hold values from -0.125 to 0.125
- w_forget: bfloat16 [2048, 2048], P('ep', 'tp'), may hold values from -0.125 to 0.125
- w_value: bfloat16 [2048, 2048], P('ep', 'tp'), may hold values from -0.125 to 0.125
- w_outgate: bfloat16 [2048, 2048], P('ep', 'tp'), may hold values from -0.125 to 0.125
- w_mix_out: bfloat16 [2048, 2048], P('tp', 'ep'), may hold values from -0.125 to 0.125
- routes: int32 [128, 2], P('ep'), may hold values from 0 to 7, all different within a row; in each aligned block of 16 rows (0 to 15, 16 to 31, ...) at most 8 rows name the same one
- route_scores: float32 [128, 2], P('ep'), may hold values from -6 to 6
- w_exp_gate: bfloat16 [8, 2048, 3584], P('ep', None, 'tp'), may hold values from -0.125 to 0.125
- w_exp_up: bfloat16 [8, 2048, 3584], P('ep', None, 'tp'), may hold values from -0.125 to 0.125
- w_exp_down: bfloat16 [8, 3584, 2048], P('ep', 'tp'), may hold values from -0.75 to 0.75
- w_dense_gate: bfloat16 [2048, 6144], P('ep', 'tp'), may hold values from -0.125 to 0.125
- w_dense_up: bfloat16 [2048, 6144], P('ep', 'tp'), may hold values from -0.125 to 0.125
- w_dense_down: bfloat16 [6144, 2048], P('tp', 'ep'), may hold values from -0.75 to 0.75
- dense_mix: bfloat16 [2048], replicated, may hold values from -0.125 to 0.125
Outputs:
- layer_out: bfloat16 [128, 2048], P('ep', 'tp')
- new_state: float32 [128, 16, 128, 128], P('ep', 'tp')
Inputs may be any that keep to these rules, and one draw needn't show every extreme that they name: `routes`: each row names 2 different experts. In each aligned block of 16 rows no expert is named by more than 8 rows, and in every draw some expert is named by exactly 8 rows of some block.
All inputs are finite; a program needn't handle non-finite values.
Results may differ from a plain program's by a relative error of at most 0.025.
Values may be sent and summed in bfloat16 or wider, within the bound.
No kernel may reach another device: no remote copies, remote signals or barrier semaphores. Data moves between devices by JAX's collectives and lax.ppermute only.
A program may use at most 64 MiB of HBM per device.

v0:
```python
import jax
import jax.numpy as jnp
from jax import lax
from jax.sharding import PartitionSpec as P

EPS = 1e-06


def rms_scale(values):
    return lax.rsqrt(jnp.mean(values * values, axis=-1, keepdims=True) + EPS)


def body(
    tokens,
    old_state,
    lower_bound,
    head_gain,
    norm_gains,
    w_query,
    w_forget,
    w_value,
    w_outgate,
    w_mix_out,
    routes,
    route_scores,
    w_exp_gate,
    w_exp_up,
    w_exp_down,
    w_dense_gate,
    w_dense_up,
    w_dense_down,
    dense_mix,
):
    highest = lax.Precision.HIGHEST
    seqs, width = tokens.shape
    column_index = lax.axis_index("tp")
    part_width = width // lax.axis_size("tp")
    resid = tokens.astype(jnp.float32)
    normed = (resid * rms_scale(resid) * norm_gains[0]).astype(jnp.bfloat16)
    in_weights = jnp.concatenate([w_query, w_forget, w_value, w_outgate], axis=1)
    mix_rows = lax.all_to_all(normed, "ep", split_axis=1, concat_axis=0, tiled=True)
    projected = lax.psum_scatter(
        jnp.dot(mix_rows, in_weights, preferred_element_type=jnp.float32).astype(jnp.bfloat16),
        "ep",
        scatter_dimension=0,
        tiled=True,
    ).astype(jnp.float32)
    query_raw, forget_raw, value, out_gate = jnp.split(projected, 4, axis=1)
    heads = old_state.shape[1]
    head_size = old_state.shape[2]
    shape_heads = (seqs, heads, head_size)
    forget = lower_bound + (1.0 - lower_bound) * jax.nn.sigmoid(forget_raw)
    key_in = (1.0 - lower_bound) * jax.nn.sigmoid(-forget_raw)
    new_state = forget.reshape(shape_heads)[..., None] * old_state + key_in.reshape(shape_heads)[
        ..., None
    ] * value.reshape(seqs, heads, 1, head_size)
    query = jax.nn.silu(query_raw).reshape(shape_heads)
    read = jnp.einsum("thk,thkv->thv", query, new_state, precision=highest)
    gated = (
        read
        * rms_scale(read)
        * head_gain.reshape(heads, head_size)
        * jax.nn.silu(out_gate).reshape(shape_heads)
    )
    mixed_heads = gated.reshape(seqs, heads * head_size).astype(jnp.bfloat16)
    mix_part = jnp.dot(
        mixed_heads,
        lax.all_gather(w_mix_out, "ep", axis=1, tiled=True),
        preferred_element_type=jnp.float32,
    ).astype(jnp.bfloat16)
    mix_part = lax.optimization_barrier(mix_part).astype(jnp.float32)
    mix_out = lax.psum(mix_part.astype(jnp.bfloat16), "tp")
    mix_wide = lax.optimization_barrier(mix_out).astype(jnp.float32)
    after_mix = resid + mix_wide * rms_scale(mix_wide) * norm_gains[1]
    ffn_in = (after_mix * rms_scale(after_mix) * norm_gains[2]).astype(jnp.bfloat16)
    experts = lax.axis_size("ep")
    topk = routes.shape[1]
    capacity = max(2, 2 * seqs * topk // experts)
    flat_routes = routes.reshape(-1)
    onehot = (flat_routes[:, None] == jnp.arange(experts, dtype=jnp.int32)[None, :]).astype(
        jnp.int32
    )
    before = jnp.cumsum(onehot, axis=0) - onehot
    slots = jnp.sum(onehot * before, axis=1)
    cells = flat_routes * capacity + slots
    placed = cells[None, :] == jnp.arange(experts * capacity, dtype=jnp.int32)[:, None]
    repeated = jnp.repeat(ffn_in, topk, axis=0)
    outgoing = jnp.dot(placed.astype(jnp.bfloat16), repeated, preferred_element_type=jnp.float32)
    outgoing = outgoing.astype(jnp.bfloat16).reshape(experts, capacity, width)
    arrived = lax.all_to_all(outgoing, "ep", split_axis=0, concat_axis=0, tiled=True)
    sources, items, _ = arrived.shape
    expert_rows = arrived.reshape(sources * items, width)
    gate_pre = jnp.dot(expert_rows, w_exp_gate[0], preferred_element_type=jnp.float32)
    up_pre = jnp.dot(expert_rows, w_exp_up[0], preferred_element_type=jnp.float32)
    hidden = (jax.nn.silu(gate_pre) * up_pre).astype(jnp.bfloat16)
    partial_rows = jnp.dot(hidden, w_exp_down[0], preferred_element_type=jnp.float32).astype(
        jnp.bfloat16
    )
    partial_rows = lax.optimization_barrier(partial_rows).astype(jnp.float32)
    partial_rows = partial_rows.reshape(sources, items, width)
    summed = lax.psum_scatter(
        partial_rows.astype(jnp.bfloat16), "tp", scatter_dimension=2, tiled=True
    )
    returned = lax.all_to_all(summed, "ep", split_axis=0, concat_axis=0, tiled=True)
    first = jax.nn.sigmoid(route_scores[:, 0] - route_scores[:, 1])
    second = jax.nn.sigmoid(route_scores[:, 1] - route_scores[:, 0])
    route_weight = jnp.stack([first, second], axis=1).reshape(-1)
    weight_table = jnp.sum(
        (placed.astype(jnp.float32) * route_weight[None, :]).reshape(
            experts * capacity, seqs, topk
        ),
        axis=2,
    )
    expert_sum = jnp.dot(
        weight_table.T,
        returned.reshape(experts * capacity, part_width).astype(jnp.float32),
        precision=highest,
    )
    dense_weights = jnp.concatenate([w_dense_gate, w_dense_up], axis=1)
    dense_rows = lax.all_to_all(ffn_in, "ep", split_axis=1, concat_axis=0, tiled=True)
    dense_pre = lax.psum_scatter(
        jnp.dot(dense_rows, dense_weights, preferred_element_type=jnp.float32).astype(jnp.bfloat16),
        "ep",
        scatter_dimension=0,
        tiled=True,
    ).astype(jnp.float32)
    dense_gate_pre, dense_up_pre = jnp.split(dense_pre, 2, axis=1)
    dense_hidden = (jax.nn.silu(dense_gate_pre) * dense_up_pre).astype(jnp.bfloat16)
    dense_partial = jnp.dot(
        dense_hidden,
        lax.all_gather(w_dense_down, "ep", axis=1, tiled=True),
        preferred_element_type=jnp.float32,
    )
    dense_out = lax.psum_scatter(
        dense_partial.astype(jnp.bfloat16), "tp", scatter_dimension=1, tiled=True
    ).astype(jnp.float32)
    mix_weight = jax.nn.sigmoid(jnp.dot(ffn_in, dense_mix, preferred_element_type=jnp.float32))
    ffn_out = expert_sum + mix_weight[:, None] * dense_out
    squares = lax.psum(jnp.sum(ffn_out * ffn_out, axis=1), "tp")
    out_scale = lax.rsqrt(squares / width + EPS)
    gain_part = lax.dynamic_slice_in_dim(norm_gains[3], column_index * part_width, part_width, 0)
    resid_part = lax.dynamic_slice_in_dim(after_mix, column_index * part_width, part_width, 1)
    layer_out = (resid_part + ffn_out * out_scale[:, None] * gain_part).astype(jnp.bfloat16)
    return (layer_out, new_state)


def solution(mesh):
    return jax.shard_map(
        body,
        mesh=mesh,
        in_specs=(
            P("ep", None),
            P("ep", "tp", None, None),
            P("tp"),
            P("tp"),
            P(),
            P("ep", "tp"),
            P("ep", "tp"),
            P("ep", "tp"),
            P("ep", "tp"),
            P("tp", "ep"),
            P("ep", None),
            P("ep", None),
            P("ep", None, "tp"),
            P("ep", None, "tp"),
            P("ep", "tp", None),
            P("ep", "tp"),
            P("ep", "tp"),
            P("tp", "ep"),
            P(),
        ),
        out_specs=(P("ep", "tp"), P("ep", "tp", None, None)),
        check_vma=False,
    )
```

profile of v0, /device:TPU:0, one launch (start us, length us, event | category | flops | bytes accessed | tf_op | source)
XLA Modules:
  0.0 319.4 jit_solution(3477213161517081613)
XLA Ops:
  7.2 0.9 fusion.58
  8.2 1.0 fusion.42
  9.2 0.9 fusion.44
  10.1 12.1 %all_to_all.48 = bf16[16,8,256]{2,0,1:T(8,128)(2,1)S(1)} all-to-all(bf16[16,8,256]{2,0,1:T(8,128)(2,1)S(1)} %bitcast.82), channel_id=1, replica_groups=mesh['ep'=8,'tp'=4] {'ep'}, dimensions={1} | all-to-all | bytes 131072 | tf_op jit(solution)/shard_map/all_to_all | solution.py:41
  22.2 2.3 convolution_convert_fusion.1
  24.5 0.7 all-gather.3.cloned.1.call-update
  25.8 28.7 %reduce-scatter.5.cloned.1.call-done = bf16[16,2048]{1,0:T(8,128)(2,1)} async-done(((bf16[128,2048]{1,0:T(8,128)(2,1)}), bf16[16,2048]{1,0:T(8,128)(2,1)}) %reduce-scatter.5.cloned.1.call-update) | async-done | bytes 65552 | tf_op jit(solution)/shard_map/reduce_scatter | solution.py:42
  54.5 0.8 convert_element_type.70
  55.4 0.7 split.26
  56.2 4.4 %multiply_add_fusion = f32[16,4,128,128]{3,2,1,0:T(8,128)S(1)} fusion(f32[16,4,128,128]{3,2,1,0:T(8,128)} %param.20, f32[16,4,128]{2,1,0:T(4,128)S(1)} %mul.223, f32[16,4,128]{2,1,0:T(4,128)S(1)} %mul.221, f32[16,4,128]{2,1,0:T(4,128)S(1)} %mul.217), kind=kLoop, calls=%fused_computation | loop fusion | flops 3145728 | bytes 8486912 | tf_op jit(solution)/shard_map/add | solution.py:54
  60.7 2.0 copy-done
  62.6 3.7 %fusion.59 = f32[16,4,1,128]{3,2,1,0:T(1,128)S(1)} fusion(f32[16,4,128,1]{2,3,1,0:T(1,128)S(1)} %bitcast.84, f32[16,4,128,128]{3,2,1,0:T(8,128)S(1)} %multiply_add_fusion), kind=kOutput, calls=%fused_computation.92 | convolution fusion | flops 12582912 | bytes 4259840 | tf_op jit(solution)/shard_map/thk,thkv->thv/dot_general | solution.py:58
  66.5 18.5 %all-gather.3.cloned.1.call-done = bf16[512,2048]{1,0:T(8,128)(2,1)} async-done(((bf16[512,256]{1,0:T(8,128)(2,1)}), bf16[512,2048]{1,0:T(8,128)(2,1)}) %all-gather.3.cloned.1.call-update) | async-done | bytes 2097168 | tf_op jit(solution)/shard_map/all_gather | solution.py:68
  85.0 2.6 convolution_convert_fusion.4
  87.7 41.1 %all-reduce.2.cloned.1.call-done = bf16[16,2048]{1,0:T(8,128)(2,1)} async-done(((bf16[16,2048]{1,0:T(8,128)(2,1)}), bf16[16,2048]{1,0:T(8,128)(2,1)}) %all-reduce.2.cloned.1.call-update) | async-done | bytes 65552 | tf_op jit(solution)/shard_map/psum | solution.py:72
  128.8 1.0 fusion.40
  129.7 1.0 multiply_reduce_fusion
  131.2 14.1 %all_to_all.49 = bf16[8,8,2048]{2,1,0:T(8,128)(2,1)S(1)} all-to-all(bf16[8,8,2048]{2,1,0:T(8,128)(2,1)S(1)} %fusion.9), channel_id=1, replica_groups=mesh['ep'=8,'tp'=4] {'ep'}, dimensions={0} | all-to-all | bytes 524288 | tf_op jit(solution)/shard_map/all_to_all | solution.py:90
  145.4 2.7 fusion.4
  148.1 5.5 %fusion.6 = bf16[64,2048]{1,0:T(8,128)(2,1)} fusion(bf16[1,896,2048]{2,1,0:T(8,128)(2,1)} %param.33, bf16[1,2048,896]{2,1,0:T(8,128)(2,1)} %param.32, bf16[8,8,2048]{2,1,0:T(8,128)(2,1)S(1)} %all_to_all.49, f32[64,896]{1,0:T(8,128)S(1)} %fusion.4), kind=kOutput, calls=%fused_computation.9 | convolution fusion | flops 470237184 | bytes 8093696 | tf_op jit(solution)/shard_map/dot_general | solution.py:96
  153.7 8.3 %all_to_all.50 = bf16[16,8,256]{2,0,1:T(8,128)(2,1)S(1)} all-to-all(bf16[16,8,256]{2,0,1:T(8,128)(2,1)S(1)} %bitcast.83), channel_id=1, replica_groups=mesh['ep'=8,'tp'=4] {'ep'}, dimensions={1} | all-to-all | bytes 131072 | tf_op jit(solution)/shard_map/all_to_all | solution.py:120
  162.0 1.3 convolution_convert_fusion
  164.2 11.9 %reduce-scatter.7.cloned.1.call-done = bf16[8,8,512]{2,1,0:T(8,128)(2,1)} async-done(((bf16[8,8,2048]{2,1,0:T(8,128)(2,1)}), bf16[8,8,512]{2,1,0:T(8,128)(2,1)}) %reduce-scatter.7.cloned.1.call-update) | async-done | bytes 65552 | tf_op jit(solution)/shard_map/reduce_scatter | solution.py:101
  176.1 4.6 %all-to-all-start.2 = ((bf16[8,8,512]{2,1,0:T(8,128)(2,1)}), bf16[8,8,512]{2,1,0:T(8,128)(2,1)S(1)}, u32[]{:S(2)}, u32[]{:S(2)}) async-start(bf16[8,8,512]{2,1,0:T(8,128)(2,1)} %reduce-scatter.7.cloned.1.call-done), calls=%async_computation.4 | async-start | bytes 131072 | tf_op jit(solution)/shard_map/all_to_all | solution.py:104
  180.8 29.5 %reduce-scatter.9.cloned.1.call-done = bf16[16,3072]{1,0:T(8,128)(2,1)} async-done(((bf16[128,3072]{1,0:T(8,128)(2,1)}), bf16[16,3072]{1,0:T(8,128)(2,1)}) %reduce-scatter.9.cloned.1.call-update) | async-done | bytes 98320 | tf_op jit(solution)/shard_map/reduce_scatter | solution.py:121
  210.3 0.9 convert_element_type.82
  211.2 63.9 %all-gather.5.cloned.1.call-done = bf16[1536,2048]{1,0:T(8,128)(2,1)} async-done(((bf16[1536,256]{1,0:T(8,128)(2,1)}), bf16[1536,2048]{1,0:T(8,128)(2,1)}) %all-gather.5.cloned.1.call-update) | async-done | bytes 6291472 | tf_op jit(solution)/shard_map/all_gather | solution.py:131
  275.1 4.3 %convolution_convert_fusion.3 = bf16[16,2048]{1,0:T(8,128)(2,1)} fusion(bf16[1536,2048]{1,0:T(8,128)(2,1)} %all-gather.5.cloned.1.call-done, f32[16,3072]{1,0:T(8,128)S(1)} %convert_element_type.82), kind=kOutput, calls=%fused_computation.12 | convolution fusion | flops 100843520 | bytes 6553600 | tf_op jit(solution)/shard_map/dot_general | solution.py:129
  279.6 22.3 %reduce-scatter.11.cloned.1.call-done = bf16[16,512]{1,0:T(8,128)(2,1)} async-done(((bf16[16,2048]{1,0:T(8,128)(2,1)}), bf16[16,512]{1,0:T(8,128)(2,1)}) %reduce-scatter.11.cloned.1.call-update) | async-done | bytes 16400 | tf_op jit(solution)/shard_map/reduce_scatter | solution.py:134
  301.9 1.0 multiply_reduce_fusion.1
  302.9 8.9 %psum.15 = f32[16]{0:T(128)S(1)} all-reduce(f32[16]{0:T(128)S(1)} %get-tuple-element.14), channel_id=1, replica_groups=mesh['ep'=8,'tp'=4] {'tp'}, use_global_device_ids=true, to_apply=%region_13.14 | all-reduce | flops 16 | bytes 128 | tf_op jit(solution)/shard_map/psum | solution.py:139
  311.8 0.7 add_convert_fusion
  (66 shorter events, 2.6 us)
Async XLA Ops:
  7.2 18.1 %copy-start.4 = (s32[16,2]{0,1:T(2,128)S(1)}, s32[16,2]{0,1:T(2,128)}, u32[]{:S(2)}) copy-start(s32[16,2]{0,1:T(2,128)} %param.29) | copy-start | bytes 388
  7.2 18.6 %copy-start.2 = (f32[512]{0:T(512)S(1)}, f32[512]{0:T(512)}, u32[]{:S(2)}) copy-start(f32[512]{0:T(512)} %param.21) | copy-start | bytes 6148
  7.2 47.3 %reduce-scatter.5.cloned.1.call-start = ((), (), s32[]{:S(2)}) async-start(), calls=%async_computation.8 | async-start | bytes 589824 | tf_op jit(solution)/shard_map/reduce_scatter | solution.py:42
  24.5 60.5 %all-gather.3.cloned.1.call-start = ((), (), s32[]{:S(2)}) async-start(), calls=%async_computation.9 | async-start | bytes 2359296 | tf_op jit(solution)/shard_map/all_gather | solution.py:68
  25.2 103.5 %all-reduce.2.cloned.1.call-start = ((), (), s32[]{:S(2)}) async-start(), calls=%async_computation.10 | async-start | bytes 131072 | tf_op jit(solution)/shard_map/psum | solution.py:72
  60.6 2.0 copy-start
  60.6 5.8 %copy-start.5 = (f32[512]{0:T(512)S(1)}, f32[512]{0:T(512)}, u32[]{:S(2)}) copy-start(f32[512]{0:T(512)} %param.22) | copy-start | bytes 6148
  60.6 69.1 %copy-start.1 = (bf16[16,2048]{1,0:T(8,128)(2,1)S(1)}, bf16[16,2048]{1,0:T(8,128)(2,1)}, u32[]{:S(2)}) copy-start(bf16[16,2048]{1,0:T(8,128)(2,1)} %param.19) | copy-start | bytes 196612
  87.6 88.5 %reduce-scatter.7.cloned.1.call-start = ((), (), s32[]{:S(2)}) async-start(), calls=%async_computation.11 | async-start | bytes 327680 | tf_op jit(solution)/shard_map/reduce_scatter | solution.py:101
  148.1 13.9 %copy-start.7 = (bf16[256,1536]{1,0:T(8,128)(2,1)S(1)}, bf16[256,1536]{1,0:T(8,128)(2,1)}, u32[]{:S(2)}) copy-start(bf16[256,1536]{1,0:T(8,128)(2,1)} %param.35) | copy-start | bytes 2359300
  148.1 13.9 %copy-start.8 = (bf16[256,1536]{1,0:T(8,128)(2,1)S(1)}, bf16[256,1536]{1,0:T(8,128)(2,1)}, u32[]{:S(2)}) copy-start(bf16[256,1536]{1,0:T(8,128)(2,1)} %param.34) | copy-start | bytes 2359300
  153.6 10.3 %copy-start.3 = (bf16[2048]{0:T(1024)(128)(2,1)S(1)}, bf16[2048]{0:T(1024)(128)(2,1)}, u32[]{:S(2)}) copy-start(bf16[2048]{0:T(1024)(128)(2,1)} %param.37) | copy-start | bytes 12292
  153.6 10.5 %copy-start.6 = (f32[16,2]{0,1:T(2,128)S(1)}, f32[16,2]{0,1:T(2,128)}, u32[]{:S(2)}) copy-start(f32[16,2]{0,1:T(2,128)} %param.30) | copy-start | bytes 388
  153.7 56.6 %reduce-scatter.9.cloned.1.call-start = ((), (), s32[]{:S(2)}) async-start(), calls=%async_computation.12 | async-start | bytes 884736 | tf_op jit(solution)/shard_map/reduce_scatter | solution.py:121
  163.3 111.8 %all-gather.5.cloned.1.call-start = ((), (), s32[]{:S(2)}) async-start(), calls=%async_computation.13 | async-start | bytes 7077888 | tf_op jit(solution)/shard_map/all_gather | solution.py:131
  176.1 103.5 %all-to-all-start.2 = ((bf16[8,8,512]{2,1,0:T(8,128)(2,1)}), bf16[8,8,512]{2,1,0:T(8,128)(2,1)S(1)}, u32[]{:S(2)}, u32[]{:S(2)}) async-start(bf16[8,8,512]{2,1,0:T(8,128)(2,1)} %reduce-scatter.7.cloned.1.call-done), calls=%async_computation.4 | async-start | bytes 131072 | tf_op jit(solution)/shard_map/all_to_all | solution.py:104
  180.7 121.2 %reduce-scatter.11.cloned.1.call-start = ((), (), s32[]{:S(2)}) async-start(), calls=%async_computation.14 | async-start | bytes 81920 | tf_op jit(solution)/shard_map/reduce_scatter | solution.py:134
Sparse Core Ops, SparseCore 0:
  24.6 29.8 reduce-scatter.4
  56.1 28.8 all-gather.2
  87.9 40.8 all-reduce.1
  153.8 22.2 reduce-scatter.6
  178.2 31.9 reduce-scatter.8
  211.7 63.3 all-gather.4
  279.6 22.2 reduce-scatter.10
where the time goes:
time: 320 us; the launch traced here: 319 us
  waiting for transfers between devices  217 us (68%)
  blocking collectives  43.4 us (14%)
  matrix products  23.7 us (7%)
  between operations  14.4 us (4%)
  other arithmetic  11.5 us (4%)
  starting transfers between devices  4.89 us (2%)
  local copies, waits for them, and re-layouts  4.25 us (1%)
    all_gather x1, waiting for transfers between devices, body(): lax.all_gather(w_dense_down, 'ep', axis=1, tiled=True)  63.9 us
    psum x1, waiting for transfers between devices, body(): mix_out = lax.psum(mix_part.astype(jnp.bfloat16), 'tp')  41.1 us
    reduce_scatter x1, waiting for transfers between devices, body(): lax.psum_scatter(jnp.dot(dense_rows, dense_weights, preferred_element_typ...  29.5 us
    reduce_scatter x1, waiting for transfers between devices, body(): lax.psum_scatter(jnp.dot(mix_rows, in_weights, preferred_element_type=jnp...  28.7 us
    reduce_scatter x1, waiting for transfers between devices, body(): lax.psum_scatter(dense_partial.astype(jnp.bfloat16), 'tp', scatter_dimens...  22.3 us
    all_gather x1, waiting for transfers between devices, body(): lax.all_gather(w_mix_out, 'ep', axis=1, tiled=True)  18.5 us
    all_to_all x1, blocking collectives, body(): lax.all_to_all(outgoing, 'ep', split_axis=0, concat_axis=0, tiled=True)  14.1 us
    all_to_all x1, blocking collectives, body(): lax.all_to_all(normed, 'ep', split_axis=1, concat_axis=0, tiled=True)  12.1 us
  transfers between devices with their start and end apart: 8, of which 7 were waited for; matrix products, arithmetic and copies ran while one was open for 5% of the time, Pallas kernels for 0%

commit v1 on v0

--- a/solution.py
+++ b/solution.py
@@ -128,7 +128,7 @@
     dense_hidden = (jax.nn.silu(dense_gate_pre) * dense_up_pre).astype(jnp.bfloat16)
     dense_partial = jnp.dot(
         dense_hidden,
-        lax.all_gather(w_dense_down, "ep", axis=1, tiled=True),
+        jnp.concatenate(lax.all_gather(w_dense_down, "ep"), axis=1),
         preferred_element_type=jnp.float32,
     )
     dense_out = lax.psum_scatter(

time: 320 us -> 330 us (1.031)
  local copies, waits for them, and re-layouts: 4.25 us -> 12.9 us
    reshape x0 -> x1, local copies, waits for them, and re-layouts: none -> 8.63 us  [body(): jnp.concatenate(lax.all_gather(w_dense_down, 'ep'), axis=1)]
  transfers between devices with their start and end apart: 8 -> 8, of which waited for: 7 -> 7; matrix products, arithmetic and copies ran while one was open for 5% -> 8% of each run, Pallas kernels for 0% -> 0%
where the time goes in v1:
time: 330 us; the launch traced here: 329 us
  waiting for transfers between devices  217 us (66%)
  blocking collectives  43.4 us (13%)
  matrix products  24.5 us (7%)
  between operations  14.4 us (4%)
  local copies, waits for them, and re-layouts  12.9 us (4%)
  other arithmetic  11.5 us (3%)
  starting transfers between devices  4.89 us (1%)
    all_gather x1, waiting for transfers between devices, body(): lax.all_gather(w_dense_down, 'ep')  63.5 us
    psum x1, waiting for transfers between devices, body(): mix_out = lax.psum(mix_part.astype(jnp.bfloat16), 'tp')  41.1 us
    reduce_scatter x1, waiting for transfers between devices, body(): lax.psum_scatter(jnp.dot(dense_rows, dense_weights, preferred_element_typ...  29.5 us
    reduce_scatter x1, waiting for transfers between devices, body(): lax.psum_scatter(jnp.dot(mix_rows, in_weights, preferred_element_type=jnp...  28.7 us
    reduce_scatter x1, waiting for transfers between devices, body(): lax.psum_scatter(dense_partial.astype(jnp.bfloat16), 'tp', scatter_dimens...  22.8 us
    all_gather x1, waiting for transfers between devices, body(): lax.all_gather(w_mix_out, 'ep', axis=1, tiled=True)  18.5 us
    all_to_all x1, blocking collectives, body(): lax.all_to_all(outgoing, 'ep', split_axis=0, concat_axis=0, tiled=True)  14.1 us
    all_to_all x1, blocking collectives, body(): lax.all_to_all(normed, 'ep', split_axis=1, concat_axis=0, tiled=True)  12.1 us
  transfers between devices with their start and end apart: 8, of which 7 were waited for; matrix products, arithmetic and copies ran while one was open for 8% of the time, Pallas kernels for 0%

profile of v1, /device:TPU:0, one launch (start us, length us, event | category | flops | bytes accessed | tf_op | source)
XLA Modules:
  0.0 328.9 jit_solution(9589377973796641024)
XLA Ops:
  7.2 0.9 fusion.58
  8.2 1.0 fusion.42
  9.2 0.9 fusion.44
  10.1 12.1 %all_to_all.48 = bf16[16,8,256]{2,0,1:T(8,128)(2,1)S(1)} all-to-all(bf16[16,8,256]{2,0,1:T(8,128)(2,1)S(1)} %bitcast.88), channel_id=1, replica_groups=mesh['ep'=8,'tp'=4] {'ep'}, dimensions={1} | all-to-all | bytes 131072 | tf_op jit(solution)/shard_map/all_to_all | solution.py:41
  22.2 2.3 convolution_convert_fusion.1
  24.5 0.7 all-gather.4.cloned.1.call-update
  25.8 28.7 %reduce-scatter.5.cloned.1.call-done = bf16[16,2048]{1,0:T(8,128)(2,1)} async-done(((bf16[128,2048]{1,0:T(8,128)(2,1)}), bf16[16,2048]{1,0:T(8,128)(2,1)}) %reduce-scatter.5.cloned.1.call-update) | async-done | bytes 65552 | tf_op jit(solution)/shard_map/reduce_scatter | solution.py:42
  54.5 0.8 convert_element_type.70
  55.4 0.7 split.26
  56.2 4.4 %multiply_add_fusion = f32[16,4,128,128]{3,2,1,0:T(8,128)S(1)} fusion(f32[16,4,128,128]{3,2,1,0:T(8,128)} %param.20, f32[16,4,128]{2,1,0:T(4,128)S(1)} %mul.223, f32[16,4,128]{2,1,0:T(4,128)S(1)} %mul.221, f32[16,4,128]{2,1,0:T(4,128)S(1)} %mul.217), kind=kLoop, calls=%fused_computation | loop fusion | flops 3145728 | bytes 8486912 | tf_op jit(solution)/shard_map/add | solution.py:54
  60.7 2.0 copy-done
  62.6 3.7 %fusion.59 = f32[16,4,1,128]{3,2,1,0:T(1,128)S(1)} fusion(f32[16,4,128,1]{2,3,1,0:T(1,128)S(1)} %bitcast.90, f32[16,4,128,128]{3,2,1,0:T(8,128)S(1)} %multiply_add_fusion), kind=kOutput, calls=%fused_computation.92 | convolution fusion | flops 12582912 | bytes 4259840 | tf_op jit(solution)/shard_map/thk,thkv->thv/dot_general | solution.py:58
  66.5 18.5 %all-gather.4.cloned.1.call-done = bf16[512,2048]{1,0:T(8,128)(2,1)} async-done(((bf16[512,256]{1,0:T(8,128)(2,1)}), bf16[512,2048]{1,0:T(8,128)(2,1)}) %all-gather.4.cloned.1.call-update) | async-done | bytes 2097168 | tf_op jit(solution)/shard_map/all_gather | solution.py:68
  85.0 2.6 convolution_convert_fusion.4
  87.7 41.1 %all-reduce.2.cloned.1.call-done = bf16[16,2048]{1,0:T(8,128)(2,1)} async-done(((bf16[16,2048]{1,0:T(8,128)(2,1)}), bf16[16,2048]{1,0:T(8,128)(2,1)}) %all-reduce.2.cloned.1.call-update) | async-done | bytes 65552 | tf_op jit(solution)/shard_map/psum | solution.py:72
  128.8 1.0 fusion.40
  129.7 1.0 multiply_reduce_fusion
  131.2 14.1 %all_to_all.49 = bf16[8,8,2048]{2,1,0:T(8,128)(2,1)S(1)} all-to-all(bf16[8,8,2048]{2,1,0:T(8,128)(2,1)S(1)} %fusion.9), channel_id=1, replica_groups=mesh['ep'=8,'tp'=4] {'ep'}, dimensions={0} | all-to-all | bytes 524288 | tf_op jit(solution)/shard_map/all_to_all | solution.py:90
  145.4 2.7 fusion.4
  148.1 5.5 %fusion.6 = bf16[64,2048]{1,0:T(8,128)(2,1)} fusion(bf16[1,896,2048]{2,1,0:T(8,128)(2,1)} %param.33, bf16[1,2048,896]{2,1,0:T(8,128)(2,1)} %param.32, bf16[8,8,2048]{2,1,0:T(8,128)(2,1)S(1)} %all_to_all.49, f32[64,896]{1,0:T(8,128)S(1)} %fusion.4), kind=kOutput, calls=%fused_computation.9 | convolution fusion | flops 470237184 | bytes 8093696 | tf_op jit(solution)/shard_map/dot_general | solution.py:96
  153.7 8.3 %all_to_all.50 = bf16[16,8,256]{2,0,1:T(8,128)(2,1)S(1)} all-to-all(bf16[16,8,256]{2,0,1:T(8,128)(2,1)S(1)} %bitcast.89), channel_id=1, replica_groups=mesh['ep'=8,'tp'=4] {'ep'}, dimensions={1} | all-to-all | bytes 131072 | tf_op jit(solution)/shard_map/all_to_all | solution.py:120
  162.0 1.3 convolution_convert_fusion
  164.2 11.9 %reduce-scatter.7.cloned.1.call-done = bf16[8,8,512]{2,1,0:T(8,128)(2,1)} async-done(((bf16[8,8,2048]{2,1,0:T(8,128)(2,1)}), bf16[8,8,512]{2,1,0:T(8,128)(2,1)}) %reduce-scatter.7.cloned.1.call-update) | async-done | bytes 65552 | tf_op jit(solution)/shard_map/reduce_scatter | solution.py:101
  176.1 4.6 %all-to-all-start.2 = ((bf16[8,8,512]{2,1,0:T(8,128)(2,1)}), bf16[8,8,512]{2,1,0:T(8,128)(2,1)S(1)}, u32[]{:S(2)}, u32[]{:S(2)}) async-start(bf16[8,8,512]{2,1,0:T(8,128)(2,1)} %reduce-scatter.7.cloned.1.call-done), calls=%async_computation.4 | async-start | bytes 131072 | tf_op jit(solution)/shard_map/all_to_all | solution.py:104
  180.8 29.5 %reduce-scatter.9.cloned.1.call-done = bf16[16,3072]{1,0:T(8,128)(2,1)} async-done(((bf16[128,3072]{1,0:T(8,128)(2,1)}), bf16[16,3072]{1,0:T(8,128)(2,1)}) %reduce-scatter.9.cloned.1.call-update) | async-done | bytes 98320 | tf_op jit(solution)/shard_map/reduce_scatter | solution.py:121
  210.3 0.9 convert_element_type.82
  211.2 63.5 %all-gather.6.cloned.1.call-done = bf16[12288,256]{1,0:T(8,128)(2,1)} async-done(((bf16[1536,256]{1,0:T(8,128)(2,1)}), bf16[12288,256]{1,0:T(8,128)(2,1)}) %all-gather.6.cloned.1.call-update) | async-done | bytes 6291472 | tf_op jit(solution)/shard_map/all_gather | solution.py:131
  274.7 8.6 %copy.49 = bf16[1536,8,256]{0,2,1:T(8,128)(2,1)} copy(bf16[1536,8,256]{2,0,1:T(8,128)(2,1)} %bitcast.82) | data formatting | bytes 12582912 | tf_op jit(solution)/shard_map/reshape | solution.py:131
  283.4 5.1 %convolution_convert_fusion.3 = bf16[16,2048]{1,0:T(8,128)(2,1)} fusion(bf16[1536,2048]{0,1:T(8,128)(2,1)} %bitcast.81, f32[16,3072]{1,0:T(8,128)S(1)} %convert_element_type.82), kind=kOutput, calls=%fused_computation.12 | convolution fusion | flops 100843520 | bytes 6553600 | tf_op jit(solution)/shard_map/dot_general | solution.py:129
  288.7 22.8 %reduce-scatter.11.cloned.1.call-done = bf16[16,512]{1,0:T(8,128)(2,1)} async-done(((bf16[16,2048]{1,0:T(8,128)(2,1)}), bf16[16,512]{1,0:T(8,128)(2,1)}) %reduce-scatter.11.cloned.1.call-update) | async-done | bytes 16400 | tf_op jit(solution)/shard_map/reduce_scatter | solution.py:134
  311.4 1.0 multiply_reduce_fusion.1
  312.4 8.9 %psum.15 = f32[16]{0:T(128)S(1)} all-reduce(f32[16]{0:T(128)S(1)} %get-tuple-element.14), channel_id=1, replica_groups=mesh['ep'=8,'tp'=4] {'tp'}, use_global_device_ids=true, to_apply=%region_13.14 | all-reduce | flops 16 | bytes 128 | tf_op jit(solution)/shard_map/psum | solution.py:139
  (67 shorter events, 3.3 us)
Async XLA Ops:
  7.2 18.1 %copy-start.4 = (s32[16,2]{0,1:T(2,128)S(1)}, s32[16,2]{0,1:T(2,128)}, u32[]{:S(2)}) copy-start(s32[16,2]{0,1:T(2,128)} %param.29) | copy-start | bytes 388
  7.2 18.6 %copy-start.2 = (f32[512]{0:T(512)S(1)}, f32[512]{0:T(512)}, u32[]{:S(2)}) copy-start(f32[512]{0:T(512)} %param.21) | copy-start | bytes 6148
  7.2 47.3 %reduce-scatter.5.cloned.1.call-start = ((), (), s32[]{:S(2)}) async-start(), calls=%async_computation.8 | async-start | bytes 589824 | tf_op jit(solution)/shard_map/reduce_scatter | solution.py:42
  24.5 60.5 %all-gather.4.cloned.1.call-start = ((), (), s32[]{:S(2)}) async-start(), calls=%async_computation.9 | async-start | bytes 2359296 | tf_op jit(solution)/shard_map/all_gather | solution.py:68
  25.2 103.5 %all-reduce.2.cloned.1.call-start = ((), (), s32[]{:S(2)}) async-start(), calls=%async_computation.10 | async-start | bytes 131072 | tf_op jit(solution)/shard_map/psum | solution.py:72
  60.6 2.0 copy-start
  60.6 5.8 %copy-start.5 = (f32[512]{0:T(512)S(1)}, f32[512]{0:T(512)}, u32[]{:S(2)}) copy-start(f32[512]{0:T(512)} %param.22) | copy-start | bytes 6148
  60.6 69.1 %copy-start.1 = (bf16[16,2048]{1,0:T(8,128)(2,1)S(1)}, bf16[16,2048]{1,0:T(8,128)(2,1)}, u32[]{:S(2)}) copy-start(bf16[16,2048]{1,0:T(8,128)(2,1)} %param.19) | copy-start | bytes 196612
  87.6 88.5 %reduce-scatter.7.cloned.1.call-start = ((), (), s32[]{:S(2)}) async-start(), calls=%async_computation.11 | async-start | bytes 327680 | tf_op jit(solution)/shard_map/reduce_scatter | solution.py:101
  148.1 13.9 %copy-start.7 = (bf16[256,1536]{1,0:T(8,128)(2,1)S(1)}, bf16[256,1536]{1,0:T(8,128)(2,1)}, u32[]{:S(2)}) copy-start(bf16[256,1536]{1,0:T(8,128)(2,1)} %param.35) | copy-start | bytes 2359300
  148.1 13.9 %copy-start.8 = (bf16[256,1536]{1,0:T(8,128)(2,1)S(1)}, bf16[256,1536]{1,0:T(8,128)(2,1)}, u32[]{:S(2)}) copy-start(bf16[256,1536]{1,0:T(8,128)(2,1)} %param.34) | copy-start | bytes 2359300
  153.6 10.3 %copy-start.3 = (bf16[2048]{0:T(1024)(128)(2,1)S(1)}, bf16[2048]{0:T(1024)(128)(2,1)}, u32[]{:S(2)}) copy-start(bf16[2048]{0:T(1024)(128)(2,1)} %param.37) | copy-start | bytes 12292
  153.6 10.5 %copy-start.6 = (f32[16,2]{0,1:T(2,128)S(1)}, f32[16,2]{0,1:T(2,128)}, u32[]{:S(2)}) copy-start(f32[16,2]{0,1:T(2,128)} %param.30) | copy-start | bytes 388
  153.7 56.6 %reduce-scatter.9.cloned.1.call-start = ((), (), s32[]{:S(2)}) async-start(), calls=%async_computation.12 | async-start | bytes 884736 | tf_op jit(solution)/shard_map/reduce_scatter | solution.py:121
  163.3 111.4 %all-gather.6.cloned.1.call-start = ((), (), s32[]{:S(2)}) async-start(), calls=%async_computation.14 | async-start | bytes 7077888 | tf_op jit(solution)/shard_map/all_gather | solution.py:131
  176.1 112.5 %all-to-all-start.2 = ((bf16[8,8,512]{2,1,0:T(8,128)(2,1)}), bf16[8,8,512]{2,1,0:T(8,128)(2,1)S(1)}, u32[]{:S(2)}, u32[]{:S(2)}) async-start(bf16[8,8,512]{2,1,0:T(8,128)(2,1)} %reduce-scatter.7.cloned.1.call-done), calls=%async_computation.4 | async-start | bytes 131072 | tf_op jit(solution)/shard_map/all_to_all | solution.py:104
  180.7 130.7 %reduce-scatter.11.cloned.1.call-start = ((), (), s32[]{:S(2)}) async-start(), calls=%async_computation.13 | async-start | bytes 81920 | tf_op jit(solution)/shard_map/reduce_scatter | solution.py:134
Sparse Core Ops, SparseCore 0:
  24.6 29.8 reduce-scatter.4
  56.1 28.8 all-gather.3
  87.9 40.8 all-reduce.1
  153.8 22.2 reduce-scatter.6
  178.2 31.9 reduce-scatter.8
  211.8 62.8 all-gather.5
  288.6 22.7 reduce-scatter.10
